TPU v7x, 32 devices: a whole 2x2x4 slice. The times are simulated.
32 devices in a mesh: fs: 8 (over z, y), tp: 4 (over x, core).
Axes of the slice: x: 2, y: 2, z: 4, core: 2. Of those that a mesh axis runs over, the one named last changes fastest.
Arguments:
- query_one: bfloat16 [5120, 1024], P('fs', 'tp'), as said below
- key_one: bfloat16 [5120, 1024], P('fs', 'tp'), as said below
- query_two: bfloat16 [5120, 1024], P('fs', 'tp'), as said below
- key_two: bfloat16 [5120, 1024], P('fs', 'tp'), as said below
- values: bfloat16 [5120, 2048], P('fs', 'tp'), may hold values from -6 to 6
- mix_ratio: float32 [8], P('tp'), may hold values from 0.3 to 0.8
- head_gain: float32 [256], replicated, may hold values from 0.1 to 1.9
- cotangent: bfloat16 [5120, 2048], P('fs', 'tp'), may hold values from -0.3125 to 0.3125
- left_roots: bfloat16 [2048, 2048], P('fs'), as said below
- right_roots: bfloat16 [2048, 256], P('tp'), as said below
- weight: float32 [2048, 2048], P('fs', 'tp'), may hold values from -3 to 3
- momentum: float32 [2048, 2048], P('fs', 'tp'), as said below
Outputs:
- update_step: float32 [2048, 2048], P('fs', 'tp')
- weight_new: float32 [2048, 2048], P('fs', 'tp')
- momentum_new: float32 [2048, 2048], P('fs', 'tp')
- weight_copy: bfloat16 [2048, 2048], P(None, 'tp')
Inputs may be any that keep to these rules, and one draw needn't show every extreme that they name: `query_one`: Real-valued. `key_one`: Real-valued. `query_two`: Real-valued. `key_two`: Real-valued. `left_roots`: Real-valued. `right_roots`: Real-valued. `momentum`: Real-valued.
All inputs are finite; a program needn't handle non-finite values.
Results may differ from a plain program's by a relative error of at most 0.0039.
Values may be sent and summed in bfloat16 or wider, within the bound.
A program may use at most 64 MiB of HBM per device.

v0:
```python
import jax
import jax.numpy as jnp
from jax import lax
from jax.sharding import PartitionSpec as P

D = 2048
HV = 2048


epsilon = 1e-06
momentum_decay = 0.8
clip_level = 0.5
weight_decay = 0.2
step_rate = 0.1


def local(
    query_one,
    key_one,
    query_two,
    key_two,
    values,
    mix_ratio,
    head_gain,
    cotangent,
    left_roots,
    right_roots,
    weight,
    momentum,
):
    local_heads = mix_ratio.shape[0]
    tok_rows = query_one.shape[0]
    key_width = query_one.shape[1] // local_heads
    value_width = values.shape[1] // local_heads
    causal = jnp.tril(jnp.ones((tok_rows, tok_rows), dtype=bool))

    def probs(query, keys):
        scores = jnp.einsum(
            "qhd,khd->hqk",
            query.reshape(tok_rows, local_heads, key_width),
            keys.reshape(tok_rows, local_heads, key_width),
            preferred_element_type=jnp.float32,
        ) * key_width ** (-0.5)
        return jax.nn.softmax(jnp.where(causal, scores, -jnp.inf), axis=-1)

    mixed = (
        probs(query_one, key_one) - mix_ratio[:, None, None] * probs(query_two, key_two)
    ).astype(jnp.bfloat16)
    head_out = jnp.einsum(
        "hqk,khd->qhd",
        mixed,
        values.reshape(tok_rows, local_heads, value_width),
        preferred_element_type=jnp.float32,
    )
    square = jnp.mean(head_out * head_out, axis=-1, keepdims=True)
    attended = (head_out * lax.rsqrt(square + epsilon) * head_gain).astype(jnp.bfloat16)
    attended = attended.reshape(tok_rows, local_heads * value_width)
    whole_cot = lax.all_gather(cotangent, "tp", axis=1, tiled=True)
    own_rows = weight.shape[0]
    own_cols = weight.shape[1]
    contract = (((0,), (0,)), ((), ()))
    right_full = right_roots.astype(jnp.float32).reshape(local_heads, value_width, value_width)
    left_rows = left_roots.astype(jnp.float32)
    columns = whole_cot
    summed = lax.psum_scatter(
        lax.dot_general(columns, attended, contract, preferred_element_type=jnp.float32),
        "fs",
        scatter_dimension=0,
        tiled=True,
    )
    columns = left_rows
    left_done = jnp.dot(
        columns,
        lax.all_gather(summed.astype(jnp.bfloat16), "fs", axis=0, tiled=True).astype(jnp.float32),
        precision=lax.Precision.HIGHEST,
        preferred_element_type=jnp.float32,
    )
    shaped = left_done.reshape(own_rows, local_heads, value_width)
    preconditioned = jnp.einsum(
        "dhc,hce->dhe", shaped, right_full, precision=lax.Precision.HIGHEST
    ).reshape(own_rows, own_cols)
    momentum_new = momentum_decay * momentum + (1.0 - momentum_decay) * preconditioned
    total = lax.psum(jnp.sum(momentum_new * momentum_new), ("fs", "tp"))
    factor = clip_level * lax.rsqrt(total / (D * HV) + epsilon)
    update_step = factor * momentum_new + weight_decay * weight
    weight_new = weight - step_rate * update_step
    weight_copy = lax.all_gather(weight_new.astype(jnp.bfloat16), "fs", axis=0, tiled=True)
    return (update_step, weight_new, momentum_new, weight_copy)


def solution(mesh):
    in_specs = (
        P("fs", "tp"),
        P("fs", "tp"),
        P("fs", "tp"),
        P("fs", "tp"),
        P("fs", "tp"),
        P("tp"),
        P(),
        P("fs", "tp"),
        P("fs", None),
        P("tp", None),
        P("fs", "tp"),
        P("fs", "tp"),
    )
    out_specs = (P("fs", "tp"), P("fs", "tp"), P("fs", "tp"), P(None, "tp"))
    return jax.shard_map(local, mesh=mesh, in_specs=in_specs, out_specs=out_specs, check_vma=False)
```

profile of v0, /device:TPU:8, one launch (start us, length us, event | category | flops | bytes accessed | tf_op | source)
XLA Modules:
  0.0 287.3 jit_solution(13814320406210839247)
XLA Ops:
  7.2 0.7 all-gather.4.cloned.1.call-update
  7.9 0.0 reduce-scatter.2.cloned.1.call-start
  8.0 1.4 copy.28
  9.4 0.1 iota_compare_fusion
  9.5 1.7 fusion.20
  11.2 2.3 fusion.15
  13.5 3.2 %fusion.31 = (f32[2,640]{1,0:T(2,128)S(1)}, f32[2,640,640]{1,2,0:T(8,128)}) fusion(f32[2,640,640]{1,2,0:T(8,128)S(1)} %fusion.20, pred[640,640]{0,1:T(8,128)(4,1)S(1)} %iota_compare_fusion), kind=kOutput, calls=%fused_computation.46 | output fusion | flops 4915839 | bytes 6968320 | tf_op jit(solution)/shard_map/sub | solution.py:44
  16.8 7.0 %multiply_reduce_fusion = (f32[640,2]{0,1:T(2,128)S(1)}, f32[640,2,256]{0,2,1:T(8,128)S(1)}) fusion(bf16[640,2,256]{0,2,1:T(8,128)(2,1)S(1)} %bitcast.49, f32[2,640,640]{1,2,0:T(8,128)} %get-tuple-element.10, f32[2]{0:T(128)S(1)} %copy-done.8, f32[2,640]{1,0:T(2,128)S(1)} %get-tuple-element.9, f32[2,640,640]{1,2,0:T(8,128)} %fusion.15, ...), kind=kOutput, calls=%fused_computation.23 | convolution fusion | flops 428280320 | bytes 8939528 | tf_op jit(solution)/shard_map/hqk,khd->qhd/dot_general | solution.py:49
  23.8 0.2 multiply_convert_fusion
  24.0 12.3 %all-gather.4.cloned.1.call-done = bf16[640,2048]{1,0:T(8,128)(2,1)} async-done(((bf16[640,512]{1,0:T(8,128)(2,1)}), bf16[640,2048]{1,0:T(8,128)(2,1)}) %all-gather.4.cloned.1.call-update) | async-done | bytes 2621456 | tf_op jit(solution)/shard_map/all_gather | solution.py:58
  36.3 5.5 %convolution_bitcast_fusion = f32[2048,512]{0,1:T(8,128)} fusion(bf16[640,512]{0,1:T(8,128)(2,1)S(1)} %bitcast.50, bf16[640,2048]{1,0:T(8,128)(2,1)} %all-gather.4.cloned.1.call-done), kind=kOutput, calls=%fused_computation.8 | convolution fusion | flops 1342177280 | bytes 7471104 | tf_op jit(solution)/shard_map/dot_general | solution.py:66
  41.8 0.0 all-gather.6.cloned.1.call-start
  41.8 89.0 %reduce-scatter.2.cloned.1.call-done = f32[256,512]{0,1:T(8,128)} async-done(((f32[2048,512]{0,1:T(8,128)}), f32[256,512]{0,1:T(8,128)}) %reduce-scatter.2.cloned.1.call-update) | async-done | bytes 524304 | tf_op jit(solution)/shard_map/reduce_scatter | solution.py:65
  130.9 1.8 convert_element_type.17
  132.7 0.0 all-gather.8.cloned.1.call-start
  132.7 48.7 %all-gather.6.cloned.1.call-done = bf16[2048,512]{0,1:T(8,128)(2,1)} async-done(((bf16[256,512]{0,1:T(8,128)(2,1)}), bf16[2048,512]{0,1:T(8,128)(2,1)}) %all-gather.6.cloned.1.call-update) | async-done | bytes 2097168 | tf_op jit(solution)/shard_map/all_gather | solution.py:74
  181.5 2.3 fusion.32
  183.8 0.5 convolution_multiply_fusion
  184.3 0.2 copy.24
  184.5 0.8 multiply_reduce_fusion.1
  185.3 41.2 %psum.7 = f32[]{:T(128)} all-reduce(f32[]{:T(128)} %get-tuple-element.7), channel_id=1, replica_groups=mesh['fs'=8,'tp'=4] {'fs','tp'}, use_global_device_ids=true, to_apply=%region_7.8 | all-reduce | flops 1 | bytes 8 | tf_op jit(solution)/shard_map/psum | solution.py:83
  227.2 1.2 fusion.30
  228.4 49.3 %all-gather.8.cloned.1.call-done = bf16[2048,512]{1,0:T(8,128)(2,1)} async-done(((bf16[256,512]{1,0:T(8,128)(2,1)}), bf16[2048,512]{1,0:T(8,128)(2,1)}) %all-gather.8.cloned.1.call-update) | async-done | bytes 2097168 | tf_op jit(solution)/shard_map/all_gather | solution.py:87
  277.8 3.0 %copy.50 = bf16[2048,512]{1,0:T(8,128)(2,1)} copy(bf16[2048,512]{1,0:T(8,128)(2,1)} %all-gather.8.cloned.1.call-done) | data formatting | bytes 4194304
  (23 shorter events, 0.1 us)
Async XLA Ops:
  7.2 174.3 %copy-start = (bf16[256,2048]{1,0:T(8,128)(2,1)S(1)}, bf16[256,2048]{1,0:T(8,128)(2,1)}, u32[]{:S(2)}) copy-start(bf16[256,2048]{1,0:T(8,128)(2,1)} %param.20) | copy-start | bytes 3145732
  7.2 4.0 %copy-start.5 = (bf16[640,256]{1,0:T(8,128)(2,1)S(1)}, bf16[640,256]{1,0:T(8,128)(2,1)}, u32[]{:S(2)}) copy-start(bf16[640,256]{1,0:T(8,128)(2,1)} %param.14) | copy-start | bytes 983044
  7.2 4.0 %copy-start.4 = (bf16[640,256]{1,0:T(8,128)(2,1)S(1)}, bf16[640,256]{1,0:T(8,128)(2,1)}, u32[]{:S(2)}) copy-start(bf16[640,256]{1,0:T(8,128)(2,1)} %param.15) | copy-start | bytes 983044
  7.2 29.1 %all-gather.4.cloned.1.call-start = ((), (), s32[]{:S(2)}) async-start(), calls=%async_computation.1 | async-start | bytes 3276800 | tf_op jit(solution)/shard_map/all_gather | solution.py:58
  7.9 122.9 %reduce-scatter.2.cloned.1.call-start = ((), (), s32[]{:S(2)}) async-start(), calls=%async_computation.2 | async-start | bytes 4718592 | tf_op jit(solution)/shard_map/reduce_scatter | solution.py:65
  13.5 3.3 %copy-start.8 = (f32[2]{0:T(128)S(1)}, f32[2]{0:T(128)}, u32[]{:S(2)}) copy-start(f32[2]{0:T(128)} %param.17) | copy-start | bytes 28
  16.8 7.1 %copy-start.7 = (f32[256]{0:T(256)S(1)}, f32[256]{0:T(256)}, u32[]{:S(2)}) copy-start(f32[256]{0:T(256)} %param.18) | copy-start | bytes 3076
  41.8 142.0 %copy-start.6 = (bf16[512,256]{1,0:T(8,128)(2,1)S(1)}, bf16[512,256]{1,0:T(8,128)(2,1)}, u32[]{:S(2)}) copy-start(bf16[512,256]{1,0:T(8,128)(2,1)} %param.21) | copy-start | bytes 786436
  41.8 139.7 %all-gather.6.cloned.1.call-start = ((), (), s32[]{:S(2)}) async-start(), calls=%async_computation.3 | async-start | bytes 2359296 | tf_op jit(solution)/shard_map/all_gather | solution.py:74
  132.7 51.8 %copy-start.3 = (f32[256,512]{1,0:T(8,128)S(1)}, f32[256,512]{1,0:T(8,128)}, u32[]{:S(2)}) copy-start(f32[256,512]{1,0:T(8,128)} %param.23) | copy-start | bytes 1572868
  132.7 145.1 %all-gather.8.cloned.1.call-start = ((), (), s32[]{:S(2)}) async-start(), calls=%async_computation.4 | async-start | bytes 2359296 | tf_op jit(solution)/shard_map/all_gather | solution.py:87
  183.8 43.4 %copy-start.2 = (f32[256,512]{1,0:T(8,128)S(1)}, f32[256,512]{1,0:T(8,128)}, u32[]{:S(2)}) copy-start(f32[256,512]{1,0:T(8,128)} %param.22) | copy-start | bytes 1572868
  185.3 95.5 %copy-start.1 = (f32[256,512]{1,0:T(8,128)}, f32[256,512]{1,0:T(8,128)S(1)}, u32[]{:S(2)}) copy-start(f32[256,512]{1,0:T(8,128)S(1)} %get-tuple-element.19) | copy-start | bytes 1572868
Sparse Core Ops, SparseCore 0:
  9.6 26.6 all-gather.3
  41.9 88.9 reduce-scatter.1
  133.5 47.9 all-gather.5
  228.6 49.1 all-gather.7
where the time goes:
time: 289 us; the launch traced here: 287 us
  waiting for transfers between devices  200 us (69%)
  blocking collectives  41.2 us (14%)
  matrix products  19.3 us (7%)
  between operations  14.6 us (5%)
  other arithmetic  7.29 us (3%)
  local copies, waits for them, and re-layouts  4.67 us (2%)
    reduce_scatter x1, waiting for transfers between devices, local(): lax.psum_scatter(lax.dot_general(columns, attended, contract, preferred_e...  89 us
    all_gather x1, waiting for transfers between devices, local(): lax.all_gather(weight_new.astype(jnp.bfloat16), 'fs', axis=0, tiled=True)  49.3 us
    all_gather x1, waiting for transfers between devices, local(): lax.all_gather(summed.astype(jnp.bfloat16), 'fs', axis=0, tiled=True)  48.7 us
    psum x1, blocking collectives, local(): total = lax.psum(jnp.sum(momentum_new * momentum_new), ('fs', 'tp'))  41.2 us
    all_gather x1, waiting for transfers between devices, local(): whole_cot = lax.all_gather(cotangent, 'tp', axis=1, tiled=True)  12.3 us
    dot_general x1, matrix products, local(): jnp.einsum('hqk,khd->qhd', mixed, values.reshape(tok_rows, local_heads, v...  7.05 us
  transfers between devices with their start and end apart: 4, of which 4 were waited for; matrix products, arithmetic and copies ran while one was open for 6% of the time, Pallas kernels for 0%

commit v1 on v0

v1 whole, which is shorter than its diff:
```python
import functools

import jax
import jax.numpy as jnp
from jax import lax
from jax.experimental import pallas as pl
from jax.experimental.pallas import tpu as pltpu
from jax.sharding import PartitionSpec as P

epsilon = 1e-06
momentum_decay = 0.8
clip_level = 0.5
weight_decay = 0.2
step_rate = 0.1
MESH = pl.DeviceIdType.MESH


def steps(first, last, body):
    if last - first <= 8:
        for at in range(first, last):
            body(at)
    else:

        def one(at, carry):
            body(at)
            return carry

        lax.fori_loop(first, last, one, 0)


def update_kernel(n_fs, n_tp, heads, wire, *refs):
    cots = refs[:n_tp]
    (att, left, right, weight, momentum, gathered, prec, factor_ref,
     gpart, yrecv, ysum, zrecv, acc, gfull, mnew, sq_all,
     ys, yr, zs, zr, gzs, gzr, gys, gyr, wzs, wzr, wys, wyr, ss, sr) = refs[n_tp:]
    f = lax.axis_index("fs")
    t = lax.axis_index("tp")
    ny = 2
    nz = n_fs // ny
    z = f // ny
    y = f % ny
    other = 1 - y
    rows = left.shape[0]
    depth = left.shape[1]
    vw = right.shape[1]
    block = cots[0].shape[0]
    f32 = jnp.float32

    def flip(a, b):
        out, bit = 0, 1
        while bit < n_tp:
            out = out + bit * ((a // bit + b // bit) % 2)
            bit *= 2
        return out

    def part_rows(dest):
        start = dest * rows
        j = start // block
        return pl.ds(pl.multiple_of(flip(j, t) * block + (start - j * block), rows), rows)

    def rows_of(dest):
        return pl.ds(pl.multiple_of(dest * rows, rows), rows)

    def copy(src, dst, send, recv, fs):
        return pltpu.make_async_remote_copy(
            src_ref=src, dst_ref=dst, send_sem=send, recv_sem=recv, device_id={"fs": fs}, device_id_type=MESH
        )

    partner = z * ny + other

    def y_copy(h, zz):
        return copy(gpart.at[h, part_rows(zz * ny + other)], yrecv.at[h, zz], ys.at[h, zz], yr.at[h, zz], partner)

    def z_copy(h, zz, slot):
        return copy(ysum.at[h, zz], zrecv.at[h, slot], zs.at[h, zz], zr.at[h, slot], zz * ny + y)

    for h in range(heads):
        cols = pl.ds(h * vw, vw)
        for k in range(n_tp):
            gpart[h, pl.ds(k * block, block), :] = jnp.dot(
                cots[k][...], att[:, cols], preferred_element_type=f32
            ).astype(wire)
        steps(1, nz + 1, lambda s, h=h: y_copy(h, (z + s) % nz).start())

    for h in range(heads):

        def pair(s, h=h):
            zz = (z + s) % nz
            y_copy(h, zz).wait_recv()
            total = gpart[h, part_rows(zz * ny + y), :].astype(f32) + yrecv[h, zz].astype(f32)
            ysum[h, zz] = total.astype(wire)
            z_copy(h, zz, z).start()

        steps(1, nz, pair)
        y_copy(h, z).wait_recv()
        acc[h] = gpart[h, part_rows(f), :].astype(f32) + yrecv[h, z].astype(f32)

    def gather_z(buf, send, recv, h, zz, owner):
        own = buf.at[h, rows_of(owner * ny + y)]
        return copy(own, own, send.at[h, zz], recv.at[h, owner], zz * ny + y)

    def gather_y(buf, send, recv, h, owner, side):
        own = buf.at[h, rows_of(owner * ny + side)]
        return copy(own, own, send.at[h, owner], recv.at[h, owner], partner)

    def gather_start(buf, zsend, zrec, ysend, yrec, h):
        steps(1, nz, lambda s: gather_z(buf, zsend, zrec, h, (z + s) % nz, z).start())
        gather_y(buf, ysend, yrec, h, z, y).start()

    def gather_forward(buf, zsend, zrec, ysend, yrec, h):
        def one(s):
            zz = (z + s) % nz
            gather_z(buf, zsend, zrec, h, zz, zz).wait_recv()
            gather_y(buf, ysend, yrec, h, zz, y).start()

        steps(1, nz, one)

    def gather_wait(buf, zsend, zrec, ysend, yrec, h):
        steps(0, nz, lambda zz: gather_y(buf, ysend, yrec, h, zz, other).wait_recv())

    def gather_sent(buf, zsend, zrec, ysend, yrec, h):
        steps(1, nz, lambda s: gather_z(buf, zsend, zrec, h, (z + s) % nz, z).wait_send())
        steps(0, nz, lambda zz: gather_y(buf, ysend, yrec, h, zz, y).wait_send())

    gsems = (gzs, gzr, gys, gyr)
    wsems = (wzs, wzr, wys, wyr)
    for h in range(heads):

        def arrive(s, h=h):
            zz = (z + s) % nz
            z_copy(h, zz, zz).wait_recv()
            acc[h] += zrecv[h, zz].astype(f32)

        steps(1, nz, arrive)
        gfull[h, rows_of(f), :] = acc[h].astype(jnp.bfloat16)
        gather_start(gfull, *gsems, h)
    for h in range(heads):
        gather_forward(gfull, *gsems, h)

    square = jnp.zeros((1, vw), f32)
    for h in range(heads):
        cols = pl.ds(h * vw, vw)
        gather_wait(gfull, *gsems, h)
        done = jnp.dot(left[...], gfull[h], preferred_element_type=f32)
        high = done.astype(jnp.bfloat16)
        low = (done - high.astype(f32)).astype(jnp.bfloat16)
        root = right[pl.ds(h * vw, vw), :]
        made = jnp.dot(high, root, preferred_element_type=f32) + jnp.dot(low, root, preferred_element_type=f32)
        prec[:, cols] = made
        new = momentum_decay * momentum[:, cols] + (1.0 - momentum_decay) * made
        mnew[h] = new
        square = square + jnp.sum(new * new, axis=0, keepdims=True)

    n = n_fs * n_tp
    me = f * n_tp + t
    sq_all[me] = square

    def sq_copy(dest, owner):
        return pltpu.make_async_remote_copy(
            src_ref=sq_all.at[owner], dst_ref=sq_all.at[owner], send_sem=ss.at[dest], recv_sem=sr.at[owner],
            device_id={"fs": dest // n_tp, "tp": dest % n_tp}, device_id_type=MESH,
        )

    def each(body):
        def one(s, carry):
            body((me + s) % n)
            return carry

        lax.fori_loop(1, n, one, 0)

    each(lambda d: sq_copy(d, me).start())
    each(lambda d: sq_copy(d, d).wait_recv())
    total = jnp.sum(jnp.sum(sq_all[...], axis=0), axis=1, keepdims=True)
    entries = depth * heads * vw * n_tp
    factor = clip_level * lax.rsqrt(jnp.broadcast_to(total, (1, vw)) / entries + epsilon)
    factor_ref[...] = factor

    for h in range(heads):
        kept = weight[:, pl.ds(h * vw, vw)]
        step = factor * mnew[h] + weight_decay * kept
        gathered[h, rows_of(f), :] = (kept - step_rate * step).astype(jnp.bfloat16)
        gather_start(gathered, *wsems, h)
    for h in range(heads):
        gather_forward(gathered, *wsems, h)
    for h in range(heads):
        gather_wait(gathered, *wsems, h)
        steps(0, nz, lambda zz, h=h: y_copy(h, zz).wait_send())
        steps(1, nz, lambda s, h=h: z_copy(h, (z + s) % nz, z).wait_send())
        gather_sent(gfull, *gsems, h)
        gather_sent(gathered, *wsems, h)
    each(lambda d: sq_copy(d, me).wait_send())


def local(
    n_fs,
    n_tp,
    query_one,
    key_one,
    query_two,
    key_two,
    values,
    mix_ratio,
    head_gain,
    cotangent,
    left_roots,
    right_roots,
    weight,
    momentum,
):
    local_heads = mix_ratio.shape[0]
    tok_rows = query_one.shape[0]
    key_width = query_one.shape[1] // local_heads
    value_width = values.shape[1] // local_heads
    causal = jnp.tril(jnp.ones((tok_rows, tok_rows), dtype=bool))

    cots = {0: cotangent.T}
    bit = n_tp // 2
    while bit:
        perm = [(i, i ^ bit) for i in range(n_tp)]
        cots.update({k ^ bit: lax.ppermute(block, "tp", perm) for k, block in cots.items()})
        bit //= 2

    def probs(query, keys):
        scores = jnp.einsum(
            "qhd,khd->hqk",
            query.reshape(tok_rows, local_heads, key_width),
            keys.reshape(tok_rows, local_heads, key_width),
            preferred_element_type=jnp.float32,
        ) * key_width ** (-0.5)
        return jax.nn.softmax(jnp.where(causal, scores, -jnp.inf), axis=-1)

    mixed = (
        probs(query_one, key_one) - mix_ratio[:, None, None] * probs(query_two, key_two)
    ).astype(jnp.bfloat16)
    head_out = jnp.einsum(
        "hqk,khd->qhd",
        mixed,
        values.reshape(tok_rows, local_heads, value_width),
        preferred_element_type=jnp.float32,
    )
    square = jnp.mean(head_out * head_out, axis=-1, keepdims=True)
    attended = (head_out * lax.rsqrt(square + epsilon) * head_gain).astype(jnp.bfloat16)
    attended = attended.reshape(tok_rows, local_heads * value_width)

    rows, depth = left_roots.shape
    nz = n_fs // 2
    n = n_fs * n_tp
    wire = jnp.bfloat16 if n_fs <= 8 else jnp.float32
    vmem = pl.BlockSpec(memory_space=pltpu.VMEM)
    bf16, f32 = jnp.bfloat16, jnp.float32
    dma = pltpu.SemaphoreType.DMA
    gathered, prec, factor = pl.pallas_call(
        functools.partial(update_kernel, n_fs, n_tp, local_heads, wire),
        out_shape=(
            jax.ShapeDtypeStruct((local_heads, depth, value_width), bf16),
            jax.ShapeDtypeStruct(weight.shape, f32),
            jax.ShapeDtypeStruct((1, value_width), f32),
        ),
        in_specs=[vmem] * (n_tp + 5),
        out_specs=(vmem, vmem, vmem),
        scratch_shapes=[
            pltpu.VMEM((local_heads, depth, value_width), wire),
            pltpu.VMEM((local_heads, nz, rows, value_width), wire),
            pltpu.VMEM((local_heads, nz, rows, value_width), wire),
            pltpu.VMEM((local_heads, nz, rows, value_width), wire),
            pltpu.VMEM((local_heads, rows, value_width), f32),
            pltpu.VMEM((local_heads, depth, value_width), bf16),
            pltpu.VMEM((local_heads, rows, value_width), f32),
            pltpu.VMEM((n, 1, value_width), f32),
        ]
        + [dma((local_heads, nz))] * 12
        + [dma((n,))] * 2,
        compiler_params=pltpu.CompilerParams(has_side_effects=True, vmem_limit_bytes=56 * 1024 * 1024),
    )(*[cots[k] for k in range(n_tp)], attended, left_roots, right_roots, weight, momentum)
    factor = factor[:1, :1]
    momentum_new = momentum_decay * momentum + (1.0 - momentum_decay) * prec
    update_step = factor * momentum_new + weight_decay * weight
    weight_new = weight - step_rate * update_step
    weight_copy = jnp.swapaxes(gathered, 0, 1).reshape(depth, local_heads * value_width)
    return (update_step, weight_new, momentum_new, weight_copy)


def solution(mesh):
    in_specs = (
        P("fs", "tp"),
        P("fs", "tp"),
        P("fs", "tp"),
        P("fs", "tp"),
        P("fs", "tp"),
        P("tp"),
        P(),
        P("fs", "tp"),
        P("fs", None),
        P("tp", None),
        P("fs", "tp"),
        P("fs", "tp"),
    )
    out_specs = (P("fs", "tp"), P("fs", "tp"), P("fs", "tp"), P(None, "tp"))
    body = functools.partial(local, mesh.shape["fs"], mesh.shape["tp"])
    return jax.shard_map(body, mesh=mesh, in_specs=in_specs, out_specs=out_specs, check_vma=False)
```

time: 289 us -> 158 us (0.55)
  waiting for transfers between devices: 200 us -> 6.4 us
  Pallas kernels: 0 us -> 122 us
  blocking collectives: 41.2 us -> 0 us
  between operations: 14.6 us -> 0.75 us
  matrix products: 19.3 us -> 10.2 us
  local copies, waits for them, and re-layouts: 4.67 us -> 10.7 us
    pallas_call x0 -> x1, Pallas kernels: none -> 122 us  [local(): pl.pallas_call(functools.partial(update_kernel, n_fs, n_tp, local_heads,...]
    all_gather x3 -> x0, waiting for transfers between devices: 110 us -> none  [the longest x1 49.3 us: local(): lax.all_gather(weight_new.astype(jnp.bfloat16), 'fs', axis=0, tiled=True)]
    reduce_scatter x1 -> x0, waiting for transfers between devices: 89 us -> none  [local(): lax.psum_scatter(lax.dot_general(columns, attended, contract, preferred_e...]
    psum x1 -> x0, blocking collectives: 41.2 us -> none  [local(): total = lax.psum(jnp.sum(momentum_new * momentum_new), ('fs', 'tp'))]
    dot_general x3 -> x0, matrix products: 8.28 us -> none  [the longest x1 5.47 us: local(): lax.dot_general(columns, attended, contract, preferred_element_type=jnp.f...]
    ppermute x0 -> x3, waiting for transfers between devices: none -> 6.4 us  [local(): lax.ppermute(block, 'tp', perm)]
    transpose x0 -> x1, local copies, waits for them, and re-layouts: none -> 3.02 us  [local(): jnp.swapaxes(gathered, 0, 1).reshape(depth, local_heads * value_width)]
    sub x0 -> x1, other arithmetic: none -> 2.99 us  [local(): weight_new = weight - step_rate * update_step]
  transfers between devices with their start and end apart: 4 -> 3, of which waited for: 4 -> 1; matrix products, arithmetic and copies ran while one was open for 6% -> 10% of each run, Pallas kernels for 0% -> 0%
where the time goes in v1:
time: 158 us
  Pallas kernels  122 us (77%)
  local copies, waits for them, and re-layouts  10.7 us (7%)
  matrix products  10.2 us (6%)
  other arithmetic  6.54 us (4%)
  waiting for transfers between devices  6.4 us (4%)
    pallas_call x1, Pallas kernels, local(): pl.pallas_call(functools.partial(update_kernel, n_fs, n_tp, local_heads,...  122 us
    ppermute x3, waiting for transfers between devices, local(): lax.ppermute(block, 'tp', perm)  6.4 us
    dot_general x1, matrix products, local(): jnp.einsum('hqk,khd->qhd', mixed, values.reshape(tok_rows, local_heads, v...  6.32 us
    unnamed x18, local copies, waits for them, and re-layouts  4 us
    dot_general x2, matrix products, probs(): jnp.einsum('qhd,khd->hqk', query.reshape(tok_rows, local_heads, key_width...  3.88 us
    sub x1, other arithmetic, probs(): return jax.nn.softmax(jnp.where(causal, scores, -jnp.inf), axis=-1)  3.26 us
  transfers between devices with their start and end apart: 3, of which 1 were waited for; matrix products, arithmetic and copies ran while one was open for 10% of the time, Pallas kernels for 0%

profile of v1, /device:TPU:8, one launch (start us, length us, event | category | flops | bytes accessed | tf_op | source)
XLA Modules:
  0.0 157.8 jit_solution(13264083609712853525)
XLA Ops:
  0.6 0.0 copy-start
  0.6 0.0 copy-start.5
  0.7 1.5 copy.24
  2.1 0.0 copy-start.1
  2.1 1.6 collective-permute-start.1
  3.7 0.0 collective-permute-start
  3.7 0.1 iota_compare_fusion
  3.8 1.4 copy.35
  5.2 1.6 fusion.20
  6.8 2.3 %fusion.15 = f32[2,640,640]{1,2,0:T(8,128)} fusion(bf16[640,256]{1,0:T(8,128)(2,1)S(1)} %copy-done.4, bf16[640,256]{1,0:T(8,128)(2,1)S(1)} %copy-done.5), kind=kOutput, calls=%fused_computation.26 | convolution fusion | flops 209715200 | bytes 3932160 | tf_op jit(solution)/shard_map/qhd,khd->hqk/dot_general | solution.py:224
  9.1 3.3 %fusion.30 = (f32[2,640]{1,0:T(2,128)S(1)}, f32[2,640,640]{1,2,0:T(8,128)}) fusion(f32[2,640,640]{1,2,0:T(8,128)S(1)} %fusion.20, pred[640,640]{0,1:T(8,128)(4,1)S(1)} %iota_compare_fusion), kind=kOutput, calls=%fused_computation.42 | output fusion | flops 4915839 | bytes 6968320 | tf_op jit(solution)/shard_map/sub | solution.py:230
  12.4 6.4 %collective-permute-done.1.refs_2_ = bf16[512,640]{1,0:T(8,128)(2,1)} collective-permute-done((bf16[512,640]{1,0:T(8,128)(2,1)S(1)}, bf16[512,640]{1,0:T(8,128)(2,1)}, u32[]{:S(2)}, u32[]{:S(2)}) %collective-permute-start.1) | collective-permute-done | bytes 655392 | tf_op jit(solution)/shard_map/ppermute | solution.py:220
  18.8 0.0 collective-permute-start.2
  18.8 6.3 %multiply_reduce_fusion = (f32[640,2]{0,1:T(2,128)S(1)}, f32[640,2,256]{0,2,1:T(8,128)S(1)}) fusion(bf16[640,2,256]{0,2,1:T(8,128)(2,1)S(1)} %bitcast.43, f32[2,640,640]{1,2,0:T(8,128)} %get-tuple-element.18, f32[2]{0:T(128)S(1)} %copy-done.7, f32[2,640]{1,0:T(2,128)S(1)} %get-tuple-element.17, f32[2,640,640]{1,2,0:T(8,128)} %fusion.15, ...), kind=kOutput, calls=%fused_computation.22 | convolution fusion | flops 428280320 | bytes 8939528 | tf_op jit(solution)/shard_map/hqk,khd->qhd/dot_general | solution.py:235
  25.1 0.2 multiply_convert_fusion
  25.3 1.1 copy.36.refs_4_
  26.4 0.0 collective-permute-done.refs_1_
  26.4 0.0 collective-permute-done.2.refs_3_
  26.4 121.7 %shard_map.147 = (bf16[2,2048,256]{2,1,0:T(8,128)(2,1)}, f32[256,512]{1,0:T(8,128)}, f32[1,256]{1,0:T(1,128)}) custom-call(bf16[512,640]{1,0:T(8,128)(2,1)} %bitcast.41, bf16[512,640]{1,0:T(8,128)(2,1)} %collective-permute-done.refs_1_, bf16[512,640]{1,0:T(8,128)(2,1)} %collective-permute-done.1.refs_2_, bf16[512,640]{1,0:T(8,128)(2,1)} %collective-permute-done.2.refs_3_, ...), custom_call_target="tpu_custom_call" | custom-call | tf_op jit(solution)/shard_map/pallas_call | solution.py:252
  148.1 1.2 slice.3
  149.3 3.0 %copy.32 = bf16[2048,2,256]{0,2,1:T(8,128)(2,1)S(1)} copy(bf16[2048,2,256]{2,0,1:T(8,128)(2,1)} %bitcast.42) | data formatting | bytes 4194304 | tf_op jit(solution)/shard_map/transpose | solution.py:279
  152.3 2.5 %copy.33 = bf16[2048,512]{1,0:T(8,128)(2,1)} copy(bf16[2048,512]{0,1:T(8,128)(2,1)S(1)} %bitcast.37) | data formatting | bytes 4194304
  154.8 0.0 copy-done.2
  154.9 3.0 %multiply_subtract_fusion = (f32[256,512]{1,0:T(8,128)}, f32[256,512]{1,0:T(8,128)}, f32[256,512]{1,0:T(8,128)}) fusion(f32[256,512]{1,0:T(8,128)S(1)} %copy-done.2, f32[]{:T(128)} %bitcast.4, f32[256,512]{1,0:T(8,128)} %get-tuple-element.8, f32[256,512]{1,0:T(8,128)S(1)} %copy-done.3), kind=kLoop, calls=%fused_computation.23 | loop fusion | flops 1048576 | bytes 3145732 | tf_op jit(solution)/shard_map/sub | solution.py:278
  (13 shorter events, 0.0 us)
Async XLA Ops:
  0.6 4.6 %copy-start = (bf16[640,256]{1,0:T(8,128)(2,1)S(1)}, bf16[640,256]{1,0:T(8,128)(2,1)}, u32[]{:S(2)}) copy-start(bf16[640,256]{1,0:T(8,128)(2,1)} %param.13) | copy-start | bytes 983044
  0.6 6.1 %copy-start.5 = (bf16[640,256]{1,0:T(8,128)(2,1)S(1)}, bf16[640,256]{1,0:T(8,128)(2,1)}, u32[]{:S(2)}) copy-start(bf16[640,256]{1,0:T(8,128)(2,1)} %param.14) | copy-start | bytes 983044
  0.7 6.1 %copy-start.4 = (bf16[640,256]{1,0:T(8,128)(2,1)S(1)}, bf16[640,256]{1,0:T(8,128)(2,1)}, u32[]{:S(2)}) copy-start(bf16[640,256]{1,0:T(8,128)(2,1)} %param.15) | copy-start | bytes 983044
  2.1 7.0 %copy-start.1 = (bf16[640,512]{0,1:T(8,128)(2,1)}, bf16[640,512]{0,1:T(8,128)(2,1)S(1)}, u32[]{:S(2)}) copy-start(bf16[640,512]{0,1:T(8,128)(2,1)S(1)} %copy.24) | copy-start | bytes 1966084
  2.1 16.6 %collective-permute-start.1 = (bf16[512,640]{1,0:T(8,128)(2,1)S(1)}, bf16[512,640]{1,0:T(8,128)(2,1)}, u32[]{:S(2)}, u32[]{:S(2)}) collective-permute-start(bf16[512,640]{1,0:T(8,128)(2,1)S(1)} %bitcast.39), channel_id=1, source_target_pairs={{0,2},{1,3},{2,0},{3,1},{4,6},{5,7},{6,4},{7,5},{8,10},{9,11},{10,... | collective-permute-start | bytes 1966088 | tf_op jit(solution)/shard_map/ppermute | solution.py:220
  3.7 22.7 %collective-permute-start = (bf16[512,640]{1,0:T(8,128)(2,1)S(1)}, bf16[512,640]{1,0:T(8,128)(2,1)}, u32[]{:S(2)}, u32[]{:S(2)}) collective-permute-start(bf16[512,640]{1,0:T(8,128)(2,1)S(1)} %bitcast.40), channel_id=1, source_target_pairs={{0,1},{1,0},{2,3},{3,2},{4,5},{5,4},{6,7},{7,6},{8,9},{9,8},{10,11... | collective-permute-start | bytes 1966088 | tf_op jit(solution)/shard_map/ppermute | solution.py:220
  9.1 9.7 %copy-start.7 = (f32[2]{0:T(128)S(1)}, f32[2]{0:T(128)}, u32[]{:S(2)}) copy-start(f32[2]{0:T(128)} %param.17) | copy-start | bytes 28
  18.8 7.7 %collective-permute-start.2 = (bf16[512,640]{1,0:T(8,128)(2,1)}, bf16[512,640]{1,0:T(8,128)(2,1)}, u32[]{:S(2)}, u32[]{:S(2)}) collective-permute-start(bf16[512,640]{1,0:T(8,128)(2,1)} %collective-permute-done.1.refs_2_), channel_id=1, source_target_pairs={{0,1},{1,0},{2,3},{3,2},{4,5},{5,4},{6,7},{7,6},{8,9},{9,8},{10,11... | collective-permute-start | bytes 1966088 | tf_op jit(solution)/shard_map/ppermute | solution.py:220
  18.8 6.3 %copy-start.6 = (f32[256]{0:T(256)S(1)}, f32[256]{0:T(256)}, u32[]{:S(2)}) copy-start(f32[256]{0:T(256)} %param.18) | copy-start | bytes 3076
  149.3 5.5 %copy-start.2 = (f32[256,512]{1,0:T(8,128)S(1)}, f32[256,512]{1,0:T(8,128)}, u32[]{:S(2)}) copy-start(f32[256,512]{1,0:T(8,128)} %refs_7_.1) | copy-start | bytes 1572868
  149.3 5.5 %copy-start.3 = (f32[256,512]{1,0:T(8,128)S(1)}, f32[256,512]{1,0:T(8,128)}, u32[]{:S(2)}) copy-start(f32[256,512]{1,0:T(8,128)} %refs_8_.1) | copy-start | bytes 1572868

commit v2 on v1

--- a/solution.py
+++ b/solution.py
@@ -29,21 +29,23 @@
 
 
 def update_kernel(n_fs, n_tp, heads, wire, *refs):
-    cots = refs[:n_tp]
-    (att, left, right, weight, momentum, gathered, prec, factor_ref,
-     gpart, yrecv, ysum, zrecv, acc, gfull, mnew, sq_all,
-     ys, yr, zs, zr, gzs, gzr, gys, gyr, wzs, wzr, wys, wyr, ss, sr) = refs[n_tp:]
+    (mix, q_one, k_one, q_two, k_two, values, gain, cot, left, right, weight, momentum,
+     gathered, prec, factor_ref,
+     att, cots, gpart, yrecv, ysum, zrecv, acc, gfull, mnew, sq_all,
+     cs, cr, ys, yr, zs, zr, gzs, gzr, gys, gyr, wzs, wzr, wys, wyr, ss, sr) = refs
     f = lax.axis_index("fs")
     t = lax.axis_index("tp")
     ny = 2
     nz = n_fs // ny
+    pz = nz // n_tp
     z = f // ny
     y = f % ny
     other = 1 - y
     rows = left.shape[0]
     depth = left.shape[1]
     vw = right.shape[1]
-    block = cots[0].shape[0]
+    block = cot.shape[0]
+    tokens = cot.shape[1]
     f32 = jnp.float32
 
     def flip(a, b):
@@ -58,6 +60,45 @@
         j = start // block
         return pl.ds(pl.multiple_of(flip(j, t) * block + (start - j * block), rows), rows)
 
+    def cot_copy(k, bit):
+        src = cot if k == 0 else cots.at[k]
+        return pltpu.make_async_remote_copy(
+            src_ref=src, dst_ref=cots.at[k + bit], send_sem=cs.at[k + bit], recv_sem=cr.at[k + bit],
+            device_id={"tp": flip(t, bit)}, device_id_type=MESH,
+        )
+
+    bits = []
+    while 2 ** len(bits) < n_tp:
+        bits.insert(0, 2 ** len(bits))
+    for bit in bits:
+        cot_copy(0, bit).start()
+
+    key_width = q_one.shape[1] // heads
+    tile = 128
+    lanes = (((1,), (1,)), ((), ()))
+
+    def attend(h):
+        kcols = pl.ds(h * key_width, key_width)
+        vcols = pl.ds(h * vw, vw)
+        for first in range(0, tokens, tile):
+            seen = first + tile
+            causal = lax.broadcasted_iota(jnp.int32, (tile, seen), 1) <= first + lax.broadcasted_iota(
+                jnp.int32, (tile, seen), 0
+            )
+
+            def probs(query, keys):
+                scores = lax.dot_general(
+                    query[pl.ds(first, tile), kcols], keys[pl.ds(0, seen), kcols], lanes, preferred_element_type=f32
+                ) * key_width ** (-0.5)
+                scores = jnp.where(causal, scores, -jnp.inf)
+                grown = jnp.exp(scores - jnp.max(scores, axis=1, keepdims=True))
+                return grown * (1.0 / jnp.sum(grown, axis=1, keepdims=True))
+
+            mixed = (probs(q_one, k_one) - mix[h] * probs(q_two, k_two)).astype(jnp.bfloat16)
+            out = jnp.dot(mixed, values[pl.ds(0, seen), vcols], preferred_element_type=f32)
+            square = jnp.mean(out * out, axis=1, keepdims=True)
+            att[pl.ds(first, tile), vcols] = (out * lax.rsqrt(square + epsilon) * gain[...]).astype(jnp.bfloat16)
+
     def rows_of(dest):
         return pl.ds(pl.multiple_of(dest * rows, rows), rows)
 
@@ -74,33 +115,85 @@
     def z_copy(h, zz, slot):
         return copy(ysum.at[h, zz], zrecv.at[h, slot], zs.at[h, zz], zr.at[h, slot], zz * ny + y)
 
-    for h in range(heads):
-        cols = pl.ds(h * vw, vw)
-        for k in range(n_tp):
-            gpart[h, pl.ds(k * block, block), :] = jnp.dot(
-                cots[k][...], att[:, cols], preferred_element_type=f32
-            ).astype(wire)
-        steps(1, nz + 1, lambda s, h=h: y_copy(h, (z + s) % nz).start())
-
-    for h in range(heads):
-
-        def pair(s, h=h):
-            zz = (z + s) % nz
+    def zz_of(k, i):
+        return flip(t, k) * pz + i
+
+    def share(h, k):
+        held = cot if k == 0 else cots.at[k]
+        gpart[h, pl.ds(k * block, block), :] = jnp.dot(
+            held[...], att[:, pl.ds(h * vw, vw)], preferred_element_type=f32
+        ).astype(wire)
+        steps(0, pz, lambda i: y_copy(h, zz_of(k, i)).start())
+
+    def pairs(h, k):
+        def pair(i):
+            zz = zz_of(k, i)
             y_copy(h, zz).wait_recv()
             total = gpart[h, part_rows(zz * ny + y), :].astype(f32) + yrecv[h, zz].astype(f32)
-            ysum[h, zz] = total.astype(wire)
-            z_copy(h, zz, z).start()
-
-        steps(1, nz, pair)
-        y_copy(h, z).wait_recv()
-        acc[h] = gpart[h, part_rows(f), :].astype(f32) + yrecv[h, z].astype(f32)
+
+            @pl.when(zz == z)
+            def _():
+                acc[h] = total
+
+            @pl.when(zz != z)
+            def _():
+                ysum[h, zz] = total.astype(wire)
+                z_copy(h, zz, z).start()
+
+        steps(0, pz, pair)
+
+    got = [0]
+
+    def need(k):
+        if k not in got:
+            got.append(k)
+            low = k & -k
+            cot_copy(k - low, low).wait_recv()
+
+    near = [0, 1]
+    for h in range(heads):
+        attend(h)
+        for k in near:
+            need(k)
+            share(h, k)
+    for k in near:
+        pairs(0, k)
+    order = list(near)
+    ready = [0]
+    for bit in bits:
+        for k in list(ready):
+            need(k)
+            if k:
+                cot_copy(k, bit).start()
+            if k not in order:
+                order.append(k)
+                for h in range(heads):
+                    share(h, k)
+            ready.append(k + bit)
+    for k in range(n_tp):
+        if k not in order:
+            order.append(k)
+            need(k)
+            for h in range(heads):
+                share(h, k)
+    for h in range(1, heads):
+        for k in near:
+            pairs(h, k)
+    for h in range(heads):
+        for k in order[len(near):]:
+            pairs(h, k)
+
+    def piece(buf, h, owner):
+        if len(buf.shape) == 3:
+            return buf.at[h, rows_of(owner)]
+        return buf.at[rows_of(owner), pl.ds(h * vw, vw)]
 
     def gather_z(buf, send, recv, h, zz, owner):
-        own = buf.at[h, rows_of(owner * ny + y)]
+        own = piece(buf, h, owner * ny + y)
         return copy(own, own, send.at[h, zz], recv.at[h, owner], zz * ny + y)
 
     def gather_y(buf, send, recv, h, owner, side):
-        own = buf.at[h, rows_of(owner * ny + side)]
+        own = piece(buf, h, owner * ny + side)
         return copy(own, own, send.at[h, owner], recv.at[h, owner], partner)
 
     def gather_start(buf, zsend, zrec, ysend, yrec, h):
@@ -173,12 +266,13 @@
     total = jnp.sum(jnp.sum(sq_all[...], axis=0), axis=1, keepdims=True)
     entries = depth * heads * vw * n_tp
     factor = clip_level * lax.rsqrt(jnp.broadcast_to(total, (1, vw)) / entries + epsilon)
-    factor_ref[...] = factor
+    for h in range(heads):
+        factor_ref[:, pl.ds(h * vw, vw)] = factor
 
     for h in range(heads):
         kept = weight[:, pl.ds(h * vw, vw)]
         step = factor * mnew[h] + weight_decay * kept
-        gathered[h, rows_of(f), :] = (kept - step_rate * step).astype(jnp.bfloat16)
+        gathered[rows_of(f), pl.ds(h * vw, vw)] = (kept - step_rate * step).astype(jnp.bfloat16)
         gather_start(gathered, *wsems, h)
     for h in range(heads):
         gather_forward(gathered, *wsems, h)
@@ -189,6 +283,11 @@
         gather_sent(gfull, *gsems, h)
         gather_sent(gathered, *wsems, h)
     each(lambda d: sq_copy(d, me).wait_send())
+    held = [0]
+    for bit in bits:
+        for k in list(held):
+            cot_copy(k, bit).wait_send()
+            held.append(k + bit)
 
 
 def local(
@@ -209,38 +308,8 @@
 ):
     local_heads = mix_ratio.shape[0]
     tok_rows = query_one.shape[0]
-    key_width = query_one.shape[1] // local_heads
     value_width = values.shape[1] // local_heads
-    causal = jnp.tril(jnp.ones((tok_rows, tok_rows), dtype=bool))
-
-    cots = {0: cotangent.T}
-    bit = n_tp // 2
-    while bit:
-        perm = [(i, i ^ bit) for i in range(n_tp)]
-        cots.update({k ^ bit: lax.ppermute(block, "tp", perm) for k, block in cots.items()})
-        bit //= 2
-
-    def probs(query, keys):
-        scores = jnp.einsum(
-            "qhd,khd->hqk",
-            query.reshape(tok_rows, local_heads, key_width),
-            keys.reshape(tok_rows, local_heads, key_width),
-            preferred_element_type=jnp.float32,
-        ) * key_width ** (-0.5)
-        return jax.nn.softmax(jnp.where(causal, scores, -jnp.inf), axis=-1)
-
-    mixed = (
-        probs(query_one, key_one) - mix_ratio[:, None, None] * probs(query_two, key_two)
-    ).astype(jnp.bfloat16)
-    head_out = jnp.einsum(
-        "hqk,khd->qhd",
-        mixed,
-        values.reshape(tok_rows, local_heads, value_width),
-        preferred_element_type=jnp.float32,
-    )
-    square = jnp.mean(head_out * head_out, axis=-1, keepdims=True)
-    attended = (head_out * lax.rsqrt(square + epsilon) * head_gain).astype(jnp.bfloat16)
-    attended = attended.reshape(tok_rows, local_heads * value_width)
+    block = cotangent.shape[1]
 
     rows, depth = left_roots.shape
     nz = n_fs // 2
@@ -252,13 +321,15 @@
     gathered, prec, factor = pl.pallas_call(
         functools.partial(update_kernel, n_fs, n_tp, local_heads, wire),
         out_shape=(
-            jax.ShapeDtypeStruct((local_heads, depth, value_width), bf16),
+            jax.ShapeDtypeStruct((depth, weight.shape[1]), bf16),
             jax.ShapeDtypeStruct(weight.shape, f32),
-            jax.ShapeDtypeStruct((1, value_width), f32),
+            jax.ShapeDtypeStruct((1, weight.shape[1]), f32),
         ),
-        in_specs=[vmem] * (n_tp + 5),
+        in_specs=[pl.BlockSpec(memory_space=pltpu.SMEM)] + [vmem] * 11,
         out_specs=(vmem, vmem, vmem),
         scratch_shapes=[
+            pltpu.VMEM((tok_rows, weight.shape[1]), bf16),
+            pltpu.VMEM((n_tp, block, tok_rows), bf16),
             pltpu.VMEM((local_heads, depth, value_width), wire),
             pltpu.VMEM((local_heads, nz, rows, value_width), wire),
             pltpu.VMEM((local_heads, nz, rows, value_width), wire),
@@ -268,16 +339,18 @@
             pltpu.VMEM((local_heads, rows, value_width), f32),
             pltpu.VMEM((n, 1, value_width), f32),
         ]
+        + [dma((n_tp,))] * 2
         + [dma((local_heads, nz))] * 12
         + [dma((n,))] * 2,
         compiler_params=pltpu.CompilerParams(has_side_effects=True, vmem_limit_bytes=56 * 1024 * 1024),
-    )(*[cots[k] for k in range(n_tp)], attended, left_roots, right_roots, weight, momentum)
-    factor = factor[:1, :1]
+    )(
+        mix_ratio, query_one, key_one, query_two, key_two, values, head_gain.reshape(1, -1), cotangent.T,
+        left_roots, right_roots, weight, momentum,
+    )
     momentum_new = momentum_decay * momentum + (1.0 - momentum_decay) * prec
     update_step = factor * momentum_new + weight_decay * weight
     weight_new = weight - step_rate * update_step
-    weight_copy = jnp.swapaxes(gathered, 0, 1).reshape(depth, local_heads * value_width)
-    return (update_step, weight_new, momentum_new, weight_copy)
+    return (update_step, weight_new, momentum_new, gathered)
 
 
 def solution(mesh):

time: 158 us -> 142 us (0.90)
  Pallas kernels: 122 us -> 135 us
  matrix products: 10.2 us -> 0 us
  local copies, waits for them, and re-layouts: 10.7 us -> 3.49 us
  waiting for transfers between devices: 6.4 us -> 0 us
  other arithmetic: 6.54 us -> 2.53 us
    pallas_call x1, Pallas kernels: 122 us -> 135 us  [local(): pl.pallas_call(functools.partial(update_kernel, n_fs, n_tp, local_heads,...]
    dot_general x3 -> x0, matrix products: 10.2 us -> none  [the longest x1 6.32 us: local(): jnp.einsum('hqk,khd->qhd', mixed, values.reshape(tok_rows, local_heads, v...]
    ppermute x3 -> x0, waiting for transfers between devices: 6.4 us -> none  [local(): lax.ppermute(block, 'tp', perm)]
    sub x1 -> x0, other arithmetic: 3.26 us -> none  [probs(): return jax.nn.softmax(jnp.where(causal, scores, -jnp.inf), axis=-1)]
    transpose x1 -> x0, local copies, waits for them, and re-layouts: 3.02 us -> none  [local(): jnp.swapaxes(gathered, 0, 1).reshape(depth, local_heads * value_width)]
    reshape x2 -> x0, local copies, waits for them, and re-layouts: 2.49 us -> none  [the longest x1 1.38 us: local(): values.reshape(tok_rows, local_heads, value_width)]
    unnamed x18 -> x8, local copies, waits for them, and re-layouts: 4 us -> 3.49 us
  transfers between devices with their start and end apart: 3 -> 0, of which waited for: 1 -> 0; matrix products, arithmetic and copies ran while one was open for 10% -> 0% of each run, Pallas kernels for 0% -> 0%
where the time goes in v2:
time: 142 us
  Pallas kernels  135 us (95%)
  local copies, waits for them, and re-layouts  3.49 us (2%)
  other arithmetic  2.53 us (2%)
    pallas_call x1, Pallas kernels, local(): pl.pallas_call(functools.partial(update_kernel, n_fs, n_tp, local_heads,...  135 us
    unnamed x8, local copies, waits for them, and re-layouts  3.49 us

profile of v2, /device:TPU:8, one launch (start us, length us, event | category | flops | bytes accessed | tf_op | source)
XLA Modules:
  0.0 141.6 jit_solution(8692174188991402979)
XLA Ops:
  0.6 2.2 %copy.16 = bf16[640,512]{0,1:T(8,128)(2,1)} copy(bf16[640,512]{1,0:T(8,128)(2,1)} %param.19) | data formatting | bytes 1310720 | tf_op args[7]
  2.8 0.0 copy-start.1
  2.8 0.0 copy-start.2
  2.8 134.9 %shard_map.147 = (bf16[2048,512]{1,0:T(8,128)(2,1)}, f32[256,512]{1,0:T(8,128)}, f32[1,512]{1,0:T(1,128)}) custom-call(f32[2]{0:T(128)} %refs_0_.1, bf16[640,256]{1,0:T(8,128)(2,1)} %refs_1_.1, bf16[640,256]{1,0:T(8,128)(2,1)} %refs_2_.1, bf16[640,256]{1,0:T(8,128)(2,1)} %refs_3_.1, bf16[640,256]{1,0:T(8,128)(2,1)} %refs_4_.1, bf16[640,512]{1,0:T(8,128)(2,1)} %refs_5_.1, ...), custom_call_target="tpu_custom_call" | custom-call | tf_op jit(solution)/shard_map/pallas_call | solution.py:321
  137.7 0.0 copy-start
  137.7 0.0 copy-done.1
  137.7 0.0 copy-done.2
  137.7 2.5 %multiply_subtract_fusion = (f32[256,512]{1,0:T(8,128)}, f32[256,512]{1,0:T(8,128)}, f32[256,512]{1,0:T(8,128)}) fusion(f32[256,512]{1,0:T(8,128)S(1)} %copy-done.1, f32[512]{0:T(512)} %bitcast.4, f32[256,512]{1,0:T(8,128)} %get-tuple-element.8, f32[256,512]{1,0:T(8,128)S(1)} %copy-done.2), kind=kLoop, calls=%fused_computation | loop fusion | flops 1048576 | bytes 3147776 | tf_op jit(solution)/shard_map/sub | solution.py:352
  140.2 0.0 copy-done
  140.2 1.3 copy.18
Async XLA Ops:
  2.8 134.9 %copy-start.1 = (f32[256,512]{1,0:T(8,128)S(1)}, f32[256,512]{1,0:T(8,128)}, u32[]{:S(2)}) copy-start(f32[256,512]{1,0:T(8,128)} %refs_10_.1) | copy-start | bytes 1572868
  2.8 134.9 %copy-start.2 = (f32[256,512]{1,0:T(8,128)S(1)}, f32[256,512]{1,0:T(8,128)}, u32[]{:S(2)}) copy-start(f32[256,512]{1,0:T(8,128)} %refs_11_.1) | copy-start | bytes 1572868
  137.7 2.6 %copy-start = (bf16[2048,512]{1,0:T(8,128)(2,1)S(1)}, bf16[2048,512]{1,0:T(8,128)(2,1)}, u32[]{:S(2)}) copy-start(bf16[2048,512]{1,0:T(8,128)(2,1)} %get-tuple-element.20) | copy-start | bytes 6291460

commit v3 on v2

--- a/solution.py
+++ b/solution.py
@@ -31,16 +31,12 @@
 def update_kernel(n_fs, n_tp, heads, wire, *refs):
     (mix, q_one, k_one, q_two, k_two, values, gain, cot, left, right, weight, momentum,
      gathered, prec, factor_ref,
-     att, cots, gpart, yrecv, ysum, zrecv, acc, gfull, mnew, sq_all,
-     cs, cr, ys, yr, zs, zr, gzs, gzr, gys, gyr, wzs, wzr, wys, wyr, ss, sr) = refs
+     att, cots, gpart, outgoing, incoming, gfull, mnew, sq_all,
+     cs, cr, rs, rr, gs, gr, ws, wr, ss, sr) = refs
     f = lax.axis_index("fs")
     t = lax.axis_index("tp")
-    ny = 2
-    nz = n_fs // ny
-    pz = nz // n_tp
-    z = f // ny
-    y = f % ny
-    other = 1 - y
+    side = n_fs // 2
+    place = (f % 2) * (n_fs - 1 - f // 2) + (1 - f % 2) * (f // 2)
     rows = left.shape[0]
     depth = left.shape[1]
     vw = right.shape[1]
@@ -102,45 +98,92 @@
     def rows_of(dest):
         return pl.ds(pl.multiple_of(dest * rows, rows), rows)
 
-    def copy(src, dst, send, recv, fs):
+    def member(at):
+        at = (at + n_fs) % n_fs
+        back = at // side
+        return 2 * (back * (n_fs - 1 - at) + (1 - back) * at) + back
+
+    ways = ((0, 1), (1, -1))
+
+    def hops(h, d):
+        return side if (h + d) % 2 == 0 else n_fs - 1 - side
+
+    def copy(src, dst, send, recv, sign):
         return pltpu.make_async_remote_copy(
-            src_ref=src, dst_ref=dst, send_sem=send, recv_sem=recv, device_id={"fs": fs}, device_id_type=MESH
+            src_ref=src, dst_ref=dst, send_sem=send, recv_sem=recv, device_id={"fs": member(place + sign)},
+            device_id_type=MESH,
         )
 
-    partner = z * ny + other
-
-    def y_copy(h, zz):
-        return copy(gpart.at[h, part_rows(zz * ny + other)], yrecv.at[h, zz], ys.at[h, zz], yr.at[h, zz], partner)
-
-    def z_copy(h, zz, slot):
-        return copy(ysum.at[h, zz], zrecv.at[h, slot], zs.at[h, zz], zr.at[h, slot], zz * ny + y)
-
-    def zz_of(k, i):
-        return flip(t, k) * pz + i
+    def each_hop(body):
+        short = n_fs - 1 - side
+
+        def all_of(at):
+            for h in range(heads):
+                for d, sign in ways:
+                    body(h, d, sign, at)
+
+        steps(1, short, all_of)
+        for h in range(heads):
+            for d, sign in ways:
+                if hops(h, d) > short and short >= 1:
+                    body(h, d, sign, short)
+
+    def sum_copy(h, d, sign, at):
+        return copy(outgoing.at[d, h, at], incoming.at[d, h, at], rs.at[d, h, at], rr.at[d, h, at], sign)
+
+    def sum_start(h):
+        for d, sign in ways:
+            outgoing[d, h, 0] = gpart[h, part_rows(member(place + sign * hops(h, d))), :].astype(wire)
+            sum_copy(h, d, sign, 0).start()
+
+    def sum_hop(h, d, sign, at):
+        sum_copy(h, d, sign, at - 1).wait_recv()
+        own = gpart[h, part_rows(member(place + sign * (hops(h, d) - at))), :]
+        outgoing[d, h, at] = (own + incoming[d, h, at - 1].astype(f32)).astype(wire)
+        sum_copy(h, d, sign, at).start()
+
+    def sum_end(h):
+        total = gpart[h, part_rows(f), :]
+        for d, sign in ways:
+            last = hops(h, d) - 1
+            sum_copy(h, d, sign, last).wait_recv()
+            total = total + incoming[d, h, last].astype(f32)
+        return total
+
+    def piece(buf, h, owner):
+        if len(buf.shape) == 3:
+            return buf.at[h, rows_of(owner)]
+        return buf.at[rows_of(owner), pl.ds(h * vw, vw)]
+
+    def pass_copy(buf, send, recv, h, d, sign, at, back=0):
+        held = piece(buf, h, member(place - sign * (at + back)))
+        return copy(held, held, send.at[d, h, at], recv.at[d, h, at], sign)
+
+    def pass_start(buf, send, recv, h):
+        for d, sign in ways:
+            pass_copy(buf, send, recv, h, d, sign, 0).start()
+
+    def pass_rest(buf, send, recv):
+        def hop(h, d, sign, at):
+            pass_copy(buf, send, recv, h, d, sign, at - 1, 1).wait_recv()
+            pass_copy(buf, send, recv, h, d, sign, at).start()
+
+        each_hop(hop)
+
+    def pass_end(buf, send, recv, h):
+        for d, sign in ways:
+            pass_copy(buf, send, recv, h, d, sign, hops(h, d) - 1, 1).wait_recv()
+
+    def all_sent(make):
+        for h in range(heads):
+            for d, sign in ways:
+                steps(0, hops(h, d), lambda at, h=h, d=d, sign=sign: make(h, d, sign, at).wait_send())
 
     def share(h, k):
         held = cot if k == 0 else cots.at[k]
         gpart[h, pl.ds(k * block, block), :] = jnp.dot(
             held[...], att[:, pl.ds(h * vw, vw)], preferred_element_type=f32
-        ).astype(wire)
-        steps(0, pz, lambda i: y_copy(h, zz_of(k, i)).start())
-
-    def pairs(h, k):
-        def pair(i):
-            zz = zz_of(k, i)
-            y_copy(h, zz).wait_recv()
-            total = gpart[h, part_rows(zz * ny + y), :].astype(f32) + yrecv[h, zz].astype(f32)
-
-            @pl.when(zz == z)
-            def _():
-                acc[h] = total
-
-            @pl.when(zz != z)
-            def _():
-                ysum[h, zz] = total.astype(wire)
-                z_copy(h, zz, z).start()
-
-        steps(0, pz, pair)
+        )
 
     got = [0]
 
@@ -150,90 +193,30 @@
             low = k & -k
             cot_copy(k - low, low).wait_recv()
 
-    near = [0, 1]
     for h in range(heads):
         attend(h)
-        for k in near:
-            need(k)
-            share(h, k)
-    for k in near:
-        pairs(0, k)
-    order = list(near)
     ready = [0]
     for bit in bits:
         for k in list(ready):
             need(k)
             if k:
                 cot_copy(k, bit).start()
-            if k not in order:
-                order.append(k)
-                for h in range(heads):
-                    share(h, k)
             ready.append(k + bit)
-    for k in range(n_tp):
-        if k not in order:
-            order.append(k)
+    for h in range(heads):
+        for k in ready:
             need(k)
-            for h in range(heads):
-                share(h, k)
-    for h in range(1, heads):
-        for k in near:
-            pairs(h, k)
-    for h in range(heads):
-        for k in order[len(near):]:
-            pairs(h, k)
-
-    def piece(buf, h, owner):
-        if len(buf.shape) == 3:
-            return buf.at[h, rows_of(owner)]
-        return buf.at[rows_of(owner), pl.ds(h * vw, vw)]
-
-    def gather_z(buf, send, recv, h, zz, owner):
-        own = piece(buf, h, owner * ny + y)
-        return copy(own, own, send.at[h, zz], recv.at[h, owner], zz * ny + y)
-
-    def gather_y(buf, send, recv, h, owner, side):
-        own = piece(buf, h, owner * ny + side)
-        return copy(own, own, send.at[h, owner], recv.at[h, owner], partner)
-
-    def gather_start(buf, zsend, zrec, ysend, yrec, h):
-        steps(1, nz, lambda s: gather_z(buf, zsend, zrec, h, (z + s) % nz, z).start())
-        gather_y(buf, ysend, yrec, h, z, y).start()
-
-    def gather_forward(buf, zsend, zrec, ysend, yrec, h):
-        def one(s):
-            zz = (z + s) % nz
-            gather_z(buf, zsend, zrec, h, zz, zz).wait_recv()
-            gather_y(buf, ysend, yrec, h, zz, y).start()
-
-        steps(1, nz, one)
-
-    def gather_wait(buf, zsend, zrec, ysend, yrec, h):
-        steps(0, nz, lambda zz: gather_y(buf, ysend, yrec, h, zz, other).wait_recv())
-
-    def gather_sent(buf, zsend, zrec, ysend, yrec, h):
-        steps(1, nz, lambda s: gather_z(buf, zsend, zrec, h, (z + s) % nz, z).wait_send())
-        steps(0, nz, lambda zz: gather_y(buf, ysend, yrec, h, zz, y).wait_send())
-
-    gsems = (gzs, gzr, gys, gyr)
-    wsems = (wzs, wzr, wys, wyr)
-    for h in range(heads):
-
-        def arrive(s, h=h):
-            zz = (z + s) % nz
-            z_copy(h, zz, zz).wait_recv()
-            acc[h] += zrecv[h, zz].astype(f32)
-
-        steps(1, nz, arrive)
-        gfull[h, rows_of(f), :] = acc[h].astype(jnp.bfloat16)
-        gather_start(gfull, *gsems, h)
-    for h in range(heads):
-        gather_forward(gfull, *gsems, h)
+            share(h, k)
+        sum_start(h)
+    each_hop(sum_hop)
+    for h in range(heads):
+        gfull[h, rows_of(f), :] = sum_end(h).astype(jnp.bfloat16)
+        pass_start(gfull, gs, gr, h)
+    pass_rest(gfull, gs, gr)
 
     square = jnp.zeros((1, vw), f32)
     for h in range(heads):
         cols = pl.ds(h * vw, vw)
-        gather_wait(gfull, *gsems, h)
+        pass_end(gfull, gs, gr, h)
         done = jnp.dot(left[...], gfull[h], preferred_element_type=f32)
         high = done.astype(jnp.bfloat16)
         low = (done - high.astype(f32)).astype(jnp.bfloat16)
@@ -273,15 +256,13 @@
         kept = weight[:, pl.ds(h * vw, vw)]
         step = factor * mnew[h] + weight_decay * kept
         gathered[rows_of(f), pl.ds(h * vw, vw)] = (kept - step_rate * step).astype(jnp.bfloat16)
-        gather_start(gathered, *wsems, h)
-    for h in range(heads):
-        gather_forward(gathered, *wsems, h)
-    for h in range(heads):
-        gather_wait(gathered, *wsems, h)
-        steps(0, nz, lambda zz, h=h: y_copy(h, zz).wait_send())
-        steps(1, nz, lambda s, h=h: z_copy(h, (z + s) % nz, z).wait_send())
-        gather_sent(gfull, *gsems, h)
-        gather_sent(gathered, *wsems, h)
+        pass_start(gathered, ws, wr, h)
+    pass_rest(gathered, ws, wr)
+    for h in range(heads):
+        pass_end(gathered, ws, wr, h)
+    all_sent(sum_copy)
+    all_sent(functools.partial(pass_copy, gfull, gs, gr))
+    all_sent(functools.partial(pass_copy, gathered, ws, wr))
     each(lambda d: sq_copy(d, me).wait_send())
     held = [0]
     for bit in bits:
@@ -312,7 +293,7 @@
     block = cotangent.shape[1]
 
     rows, depth = left_roots.shape
-    nz = n_fs // 2
+    side = n_fs // 2
     n = n_fs * n_tp
     wire = jnp.bfloat16 if n_fs <= 8 else jnp.float32
     vmem = pl.BlockSpec(memory_space=pltpu.VMEM)
@@ -330,17 +311,15 @@
         scratch_shapes=[
             pltpu.VMEM((tok_rows, weight.shape[1]), bf16),
             pltpu.VMEM((n_tp, block, tok_rows), bf16),
-            pltpu.VMEM((local_heads, depth, value_width), wire),
-            pltpu.VMEM((local_heads, nz, rows, value_width), wire),
-            pltpu.VMEM((local_heads, nz, rows, value_width), wire),
-            pltpu.VMEM((local_heads, nz, rows, value_width), wire),
-            pltpu.VMEM((local_heads, rows, value_width), f32),
+            pltpu.VMEM((local_heads, depth, value_width), f32),
+            pltpu.VMEM((2, local_heads, side, rows, value_width), wire),
+            pltpu.VMEM((2, local_heads, side, rows, value_width), wire),
             pltpu.VMEM((local_heads, depth, value_width), bf16),
             pltpu.VMEM((local_heads, rows, value_width), f32),
             pltpu.VMEM((n, 1, value_width), f32),
         ]
         + [dma((n_tp,))] * 2
-        + [dma((local_heads, nz))] * 12
+        + [dma((2, local_heads, side))] * 6
         + [dma((n,))] * 2,
         compiler_params=pltpu.CompilerParams(has_side_effects=True, vmem_limit_bytes=56 * 1024 * 1024),
     )(

time: 142 us -> 113 us (0.80); the launches traced: 142 us -> 111 us
  Pallas kernels: 135 us -> 104 us
    pallas_call x1, Pallas kernels: 135 us -> 104 us  [local(): pl.pallas_call(functools.partial(update_kernel, n_fs, n_tp, local_heads,...]
where the time goes in v3:
time: 113 us; the launch traced here: 111 us
  Pallas kernels  104 us (92%)
  local copies, waits for them, and re-layouts  3.49 us (3%)
  other arithmetic  2.53 us (2%)
    pallas_call x1, Pallas kernels, local(): pl.pallas_call(functools.partial(update_kernel, n_fs, n_tp, local_heads,...  104 us
    unnamed x8, local copies, waits for them, and re-layouts  3.49 us
    sub x1, other arithmetic, local(): weight_new = weight - step_rate * update_step  2.53 us

profile of v3, /device:TPU:8, one launch (start us, length us, event | category | flops | bytes accessed | tf_op | source)
XLA Modules:
  0.0 110.9 jit_solution(18047144472955278607)
XLA Ops:
  0.6 2.2 %copy.16 = bf16[640,512]{0,1:T(8,128)(2,1)} copy(bf16[640,512]{1,0:T(8,128)(2,1)} %param.19) | data formatting | bytes 1310720 | tf_op args[7]
  2.8 0.0 copy-start.1
  2.8 0.0 copy-start.2
  2.8 104.2 %shard_map.147 = (bf16[2048,512]{1,0:T(8,128)(2,1)}, f32[256,512]{1,0:T(8,128)}, f32[1,512]{1,0:T(1,128)}) custom-call(f32[2]{0:T(128)} %refs_0_.1, bf16[640,256]{1,0:T(8,128)(2,1)} %refs_1_.1, bf16[640,256]{1,0:T(8,128)(2,1)} %refs_2_.1, bf16[640,256]{1,0:T(8,128)(2,1)} %refs_3_.1, bf16[640,256]{1,0:T(8,128)(2,1)} %refs_4_.1, bf16[640,512]{1,0:T(8,128)(2,1)} %refs_5_.1, ...), custom_call_target="tpu_custom_call" | custom-call | tf_op jit(solution)/shard_map/pallas_call | solution.py:302
  107.0 0.0 copy-start
  107.1 0.0 copy-done.1
  107.1 0.0 copy-done.2
  107.1 2.5 %multiply_subtract_fusion = (f32[256,512]{1,0:T(8,128)}, f32[256,512]{1,0:T(8,128)}, f32[256,512]{1,0:T(8,128)}) fusion(f32[256,512]{1,0:T(8,128)S(1)} %copy-done.1, f32[512]{0:T(512)} %bitcast.4, f32[256,512]{1,0:T(8,128)} %get-tuple-element.8, f32[256,512]{1,0:T(8,128)S(1)} %copy-done.2), kind=kLoop, calls=%fused_computation | loop fusion | flops 1048576 | bytes 3147776 | tf_op jit(solution)/shard_map/sub | solution.py:331
  109.6 0.0 copy-done
  109.6 1.3 %copy.18 = bf16[2048,512]{1,0:T(8,128)(2,1)} copy(bf16[2048,512]{1,0:T(8,128)(2,1)S(1)} %copy-done) | data formatting | bytes 4194304
Async XLA Ops:
  2.8 104.3 %copy-start.1 = (f32[256,512]{1,0:T(8,128)S(1)}, f32[256,512]{1,0:T(8,128)}, u32[]{:S(2)}) copy-start(f32[256,512]{1,0:T(8,128)} %refs_10_.1) | copy-start | bytes 1572868
  2.8 104.3 %copy-start.2 = (f32[256,512]{1,0:T(8,128)S(1)}, f32[256,512]{1,0:T(8,128)}, u32[]{:S(2)}) copy-start(f32[256,512]{1,0:T(8,128)} %refs_11_.1) | copy-start | bytes 1572868
  107.0 2.6 %copy-start = (bf16[2048,512]{1,0:T(8,128)(2,1)S(1)}, bf16[2048,512]{1,0:T(8,128)(2,1)}, u32[]{:S(2)}) copy-start(bf16[2048,512]{1,0:T(8,128)(2,1)} %get-tuple-element.20) | copy-start | bytes 6291460
